TPU v7x, 32 devices: a whole 2x2x4 slice. The times are simulated.
32 devices in a mesh: ra: 8 (over z, x), cb: 4 (over y, core).
Axes of the slice: x: 2, y: 2, z: 4, core: 2. Of those that a mesh axis runs over, the one named last changes fastest.
Arguments:
- tokens: bfloat16 [384, 4096], P(None, 'ra'), may hold values from -260 to 260
- up_weight: float32 [2, 4096, 16384], P(None, 'ra', 'cb'), may hold values from -0.125 to 0.125
- up_scale: float32 [2, 16384], P(None, 'cb'), may hold values from 0.5 to 2
- down_weight: float32 [2, 16384, 4096], P(None, 'cb', 'ra'), may hold values from -0.046875 to 0.046875
- down_scale: float32 [2, 4096], P(None, 'ra'), may hold values from 0.7 to 14
- pre_gain: float32 [2, 4096], P(None, 'ra'), may hold values from 0.1 to 1.9
- post_gain: float32 [2, 4096], P(None, 'ra'), may hold values from 0.1 to 1.9
Outputs:
- stream_out: bfloat16 [384, 4096], P(None, 'ra')
All inputs are finite; a program needn't handle non-finite values.
Results may differ from a plain program's by a relative error of at most 0.023.
Values may be sent and summed in bfloat16 or wider, within the bound.
A program may use at most 128 MiB of HBM per device.

v0:
```python
import jax
import jax.numpy as jnp
from jax import lax
from jax.sharding import PartitionSpec as P

norm_eps = 1e-06
residual_keep = 0.5


def local(tokens, up_weight, up_scale, down_weight, down_scale, pre_gain, post_gain):
    values = tokens.astype(jnp.float32)
    model_width = tokens.shape[1] * lax.axis_size("ra")
    stream = tokens
    for sublayer in range(up_weight.shape[0]):
        scaled = (values * pre_gain[sublayer][None, :]).astype(jnp.bfloat16)
        up_matrix = up_weight[sublayer].astype(jnp.bfloat16)
        down_matrix = down_weight[sublayer].astype(jnp.bfloat16)
        partial_up = jnp.dot(scaled, up_matrix, preferred_element_type=jnp.float32)
        whole_up = lax.psum(partial_up.astype(jnp.bfloat16), "ra").astype(jnp.float32)
        hidden = jnp.square(jax.nn.relu(whole_up * up_scale[sublayer][None, :])).astype(
            jnp.bfloat16
        )
        partial_down = jnp.dot(hidden, down_matrix, preferred_element_type=jnp.float32)
        summed = lax.psum(partial_down.astype(jnp.bfloat16), "cb").astype(jnp.float32)
        branch_in = summed * down_scale[sublayer][None, :]
        post_squares = lax.psum(jnp.sum(branch_in * branch_in, axis=1), "ra")
        inv_post = lax.rsqrt(post_squares / model_width + norm_eps)[:, None]
        branch = branch_in * inv_post * post_gain[sublayer][None, :]
        stream = (residual_keep * values + branch).astype(jnp.bfloat16)
        values = stream.astype(jnp.float32)
    return stream


def solution(mesh):
    return jax.shard_map(
        local,
        mesh=mesh,
        in_specs=(
            P(None, "ra"),
            P(None, "ra", "cb"),
            P(None, "cb"),
            P(None, "cb", "ra"),
            P(None, "ra"),
            P(None, "ra"),
            P(None, "ra"),
        ),
        out_specs=P(None, "ra"),
        check_vma=False,
    )
```

profile of v0, /device:TPU:0, one launch (start us, length us, event | category | flops | bytes accessed | tf_op | source)
XLA Modules:
  0.0 411.9 jit_solution(7826004567021123031)
XLA Ops:
  6.5 0.0 copy-start.4
  6.5 0.0 copy-start.2
  6.5 0.0 all-reduce.5.cloned.1.call-start
  6.5 6.5 %convert.8 = bf16[2,512,4096]{2,1,0:T(8,128)(2,1)S(1)} convert(f32[2,512,4096]{2,1,0:T(8,128)} %param.8) | non-fusion elementwise | flops 4194304 | bytes 25165824 | tf_op jit(solution)/shard_map/convert.3
  13.1 0.0 copy-done.4
  13.1 0.0 copy-start
  13.1 3.2 copy-done
  16.3 0.0 copy-done.2
  16.3 3.5 convolution_convert_fusion.1
  19.8 0.0 all-reduce.5.cloned.1.call-update
  19.8 0.0 copy-start.5
  19.8 0.0 copy-start.3
  19.9 0.0 all-reduce.7.cloned.1.call-start
  19.9 9.0 %convert.9 = bf16[2,4096,512]{2,1,0:T(8,128)(2,1)} convert(f32[2,4096,512]{2,1,0:T(8,128)} %param.10) | non-fusion elementwise | flops 4194304 | bytes 25165824 | tf_op jit(solution)/shard_map/convert.2
  28.9 0.0 copy-done.5
  28.9 0.0 copy-done.3
  29.0 122.7 %all-reduce.5.cloned.1.call-done = bf16[384,4096]{1,0:T(8,128)(2,1)} async-done(((bf16[384,4096]{1,0:T(8,128)(2,1)}), bf16[384,4096]{1,0:T(8,128)(2,1)}) %all-reduce.5.cloned.1.call-update) | async-done | bytes 3145744 | tf_op jit(solution)/shard_map/psum | solution.py:19
  151.6 0.0 copy-start.6
  151.6 5.7 %fusion.6 = bf16[384,512]{1,0:T(8,128)(2,1)} fusion(bf16[2,4096,512]{2,1,0:T(8,128)(2,1)} %convert.9, bf16[384,4096]{1,0:T(8,128)(2,1)} %all-reduce.5.cloned.1.call-done, f32[4096]{0:T(1024)S(1)} %bitcast.30), kind=kOutput, calls=%fused_computation.14 | convolution fusion | flops 1618673664 | bytes 7749632 | tf_op jit(solution)/shard_map/dot_general | solution.py:23
  157.4 0.0 all-reduce.7.cloned.1.call-update
  157.4 0.0 all-reduce.9.cloned.1.call-start
  157.4 0.0 copy-done.6
  157.4 31.9 %all-reduce.7.cloned.1.call-done = bf16[384,512]{1,0:T(8,128)(2,1)} async-done(((bf16[384,512]{1,0:T(8,128)(2,1)}), bf16[384,512]{1,0:T(8,128)(2,1)}) %all-reduce.7.cloned.1.call-update) | async-done | bytes 393232 | tf_op jit(solution)/shard_map/psum | solution.py:24
  189.4 1.2 multiply_reduce_fusion.1
  190.5 21.3 %psum.44 = f32[384]{0:T(512)S(1)} all-reduce(f32[384]{0:T(512)S(1)} %multiply_reduce_fusion.1), channel_id=1, replica_groups=mesh['ra'=8,'cb'=4] {'ra'}, use_global_device_ids=true, to_apply=%region_3.4 | all-reduce | flops 384 | bytes 3072 | tf_op jit(solution)/shard_map/psum | solution.py:26
  211.9 5.9 %convolution_convert_fusion = bf16[384,4096]{1,0:T(8,128)(2,1)} fusion(bf16[2,512,4096]{2,1,0:T(8,128)(2,1)} %copy-done, f32[512]{0:T(512)S(1)} %bitcast.34, bf16[384,512]{1,0:T(8,128)(2,1)S(1)} %copy-done.2, bf16[384,512]{1,0:T(8,128)(2,1)} %all-reduce.7.cloned.1.call-done, f32[512]{0:T(512)S(1)} %bitcast.32, f32[384]{0:T(512)S(1)} %add_rsqrt_fusion.1, ...), kind=kOutput, calls=%fused_computation.2 | convolution fusion | flops 1614348288 | bytes 8134144 | tf_op jit(solution)/shard_map/dot_general | solution.py:18
  217.8 0.0 all-reduce.9.cloned.1.call-update
  217.8 0.0 all-reduce.11.cloned.1.call-start
  217.8 125.1 %all-reduce.9.cloned.1.call-done = bf16[384,4096]{1,0:T(8,128)(2,1)} async-done(((bf16[384,4096]{1,0:T(8,128)(2,1)}), bf16[384,4096]{1,0:T(8,128)(2,1)}) %all-reduce.9.cloned.1.call-update) | async-done | bytes 3145744 | tf_op jit(solution)/shard_map/psum | solution.py:19
  342.9 0.0 copy-start.1
  342.9 5.7 %fusion.7 = bf16[384,512]{1,0:T(8,128)(2,1)} fusion(bf16[2,4096,512]{2,1,0:T(8,128)(2,1)} %convert.9, bf16[384,4096]{1,0:T(8,128)(2,1)} %all-reduce.9.cloned.1.call-done, f32[4096]{0:T(1024)S(1)} %bitcast.29), kind=kOutput, calls=%fused_computation.15 | convolution fusion | flops 1618673664 | bytes 7749632 | tf_op jit(solution)/shard_map/dot_general | solution.py:23
  348.7 0.0 all-reduce.11.cloned.1.call-update
  348.7 32.0 %all-reduce.11.cloned.1.call-done = bf16[384,512]{1,0:T(8,128)(2,1)} async-done(((bf16[384,512]{1,0:T(8,128)(2,1)}), bf16[384,512]{1,0:T(8,128)(2,1)}) %all-reduce.11.cloned.1.call-update) | async-done | bytes 393232 | tf_op jit(solution)/shard_map/psum | solution.py:24
  380.7 1.2 multiply_reduce_fusion
  381.9 21.3 %psum.47 = f32[384]{0:T(512)S(1)} all-reduce(f32[384]{0:T(512)S(1)} %multiply_reduce_fusion), channel_id=1, replica_groups=mesh['ra'=8,'cb'=4] {'ra'}, use_global_device_ids=true, to_apply=%region_7.8 | all-reduce | flops 384 | bytes 3072 | tf_op jit(solution)/shard_map/psum | solution.py:26
  403.2 0.0 copy-done.1
  403.2 2.1 fusion.12
  (6 shorter events, 0.1 us)
Async XLA Ops:
  6.5 6.5 %copy-start.4 = (f32[2,512]{1,0:T(2,128)S(1)}, f32[2,512]{1,0:T(2,128)}, u32[]{:S(2)}) copy-start(f32[2,512]{1,0:T(2,128)} %param.12) | copy-start | bytes 12292
  6.5 9.8 %copy-start.2 = (bf16[384,512]{1,0:T(8,128)(2,1)S(1)}, bf16[384,512]{1,0:T(8,128)(2,1)}, u32[]{:S(2)}) copy-start(bf16[384,512]{1,0:T(8,128)(2,1)} %param.7) | copy-start | bytes 1179652
  6.5 145.1 %all-reduce.5.cloned.1.call-start = ((), (), s32[]{:S(2)}) async-start(), calls=%async_computation | async-start | bytes 6291456 | tf_op jit(solution)/shard_map/psum | solution.py:19
  13.1 3.2 copy-start
  19.8 9.1 %copy-start.5 = (f32[2,512]{1,0:T(2,128)S(1)}, f32[2,512]{1,0:T(2,128)}, u32[]{:S(2)}) copy-start(f32[2,512]{1,0:T(2,128)} %param.11) | copy-start | bytes 12292
  19.8 9.1 %copy-start.3 = (f32[2,4096]{1,0:T(2,128)S(1)}, f32[2,4096]{1,0:T(2,128)}, u32[]{:S(2)}) copy-start(f32[2,4096]{1,0:T(2,128)} %param.9) | copy-start | bytes 98308
  19.9 169.5 %all-reduce.7.cloned.1.call-start = ((), (), s32[]{:S(2)}) async-start(), calls=%async_computation.1 | async-start | bytes 786432 | tf_op jit(solution)/shard_map/psum | solution.py:24
  151.6 5.8 %copy-start.6 = (f32[2,512]{1,0:T(2,128)S(1)}, f32[2,512]{1,0:T(2,128)}, u32[]{:S(2)}) copy-start(f32[2,512]{1,0:T(2,128)} %param.13) | copy-start | bytes 12292
  157.4 185.6 %all-reduce.9.cloned.1.call-start = ((), (), s32[]{:S(2)}) async-start(), calls=%async_computation.2 | async-start | bytes 6291456 | tf_op jit(solution)/shard_map/psum | solution.py:19
  217.8 162.9 %all-reduce.11.cloned.1.call-start = ((), (), s32[]{:S(2)}) async-start(), calls=%async_computation.3 | async-start | bytes 786432 | tf_op jit(solution)/shard_map/psum | solution.py:24
  342.9 60.3 %copy-start.1 = (bf16[384,512]{1,0:T(8,128)(2,1)S(1)}, bf16[384,512]{1,0:T(8,128)(2,1)}, u32[]{:S(2)}) copy-start(bf16[384,512]{1,0:T(8,128)(2,1)} %all-reduce.7.cloned.1.call-done) | copy-start | bytes 1179652
Sparse Core Ops, SparseCore 0:
  19.9 131.6 all-reduce.4
  157.5 31.8 all-reduce.6
  217.9 124.9 all-reduce.8
  348.8 31.8 all-reduce.10
where the time goes:
time: 412 us
  waiting for transfers between devices  312 us (76%)
  blocking collectives  42.7 us (10%)
  matrix products  20.8 us (5%)
  other arithmetic  20 us (5%)
  between operations  13.2 us (3%)
    psum x2, waiting for transfers between devices, local(): lax.psum(partial_up.astype(jnp.bfloat16), 'ra').astype(jnp.float32)  248 us
    psum x2, waiting for transfers between devices, local(): lax.psum(partial_down.astype(jnp.bfloat16), 'cb').astype(jnp.float32)  63.9 us
    psum x2, blocking collectives, local(): post_squares = lax.psum(jnp.sum(branch_in * branch_in, axis=1), 'ra')  42.7 us
    another operation x2, other arithmetic  15.5 us
    dot_general x2, matrix products, local(): jnp.dot(hidden, down_matrix, preferred_element_type=jnp.float32)  11.4 us
    dot_general x2, matrix products, local(): partial_up = jnp.dot(scaled, up_matrix, preferred_element_type=jnp.float32)  9.37 us
  transfers between devices with their start and end apart: 4, of which 4 were waited for; matrix products, arithmetic and copies ran while one was open for 2% of the time, Pallas kernels for 0%

commit v1 on v0

--- a/solution.py
+++ b/solution.py
@@ -1,13 +1,21 @@
+import functools
+
 import jax
 import jax.numpy as jnp
 from jax import lax
+from jax.experimental import pallas as pl
+from jax.experimental.pallas import tpu as pltpu
 from jax.sharding import PartitionSpec as P
 
 norm_eps = 1e-06
 residual_keep = 0.5
-
-
-def local(tokens, up_weight, up_scale, down_weight, down_scale, pre_gain, post_gain):
+MESH = pl.DeviceIdType.MESH
+FLOWS = 4
+LANES = 128
+BF16_ROWS = 16
+
+
+def plain(tokens, up_weight, up_scale, down_weight, down_scale, pre_gain, post_gain):
     values = tokens.astype(jnp.float32)
     model_width = tokens.shape[1] * lax.axis_size("ra")
     stream = tokens
@@ -31,9 +39,342 @@
     return stream
 
 
+def kernel(
+    n, m, layers,
+    tok, up, us, dn, ds, pg, qg,
+    out,
+    st_up, st_dn, wu, wd, xs, own, sendb, recvb, hid, accd, cbb, bbuf, ssq, ssall,
+    w_sem, rs_s, rs_r, ag_s, ag_r, cb_s, cb_r, ss_s, ss_r,
+):
+    f32, bf16 = jnp.float32, jnp.bfloat16
+    ra, cb = lax.axis_index("ra"), lax.axis_index("cb")
+    rows, dl = tok.shape[1], tok.shape[2]
+    fq = wu.shape[2]
+    tokens = n * rows
+
+    def wrap(i):
+        return lax.rem(i + 2 * n, n)
+
+    half, odd = lax.div(ra, 2), lax.rem(ra, 2)
+    p = half + odd * (n - 1 - 2 * half)
+
+    def ra_of(q):
+        hi = lax.div(q, n // 2)
+        return 2 * q * (1 - hi) + hi * (2 * (n - 1 - q) + 1)
+
+    right, left = ra_of(wrap(p + 1)), ra_of(wrap(p - 1))
+    order = [0, FLOWS // 2] + [1, FLOWS // 2 + 1]
+    sign = [1 if f < FLOWS // 2 else -1 for f in range(FLOWS)]
+    target = [right if f < FLOWS // 2 else left for f in range(FLOWS)]
+
+    def up_copy(l, f):
+        return pltpu.make_async_copy(
+            up.at[l, :, pl.ds(f * fq, fq)], st_up.at[f], w_sem.at[0, f]
+        )
+
+    def dn_copy(l, f):
+        return pltpu.make_async_copy(
+            dn.at[l, pl.ds(f * fq, fq), :], st_dn.at[f], w_sem.at[1, f]
+        )
+
+    def convert(src, dst, f, block):
+        def body(i, _):
+            r = pl.ds(pl.multiple_of(i * block, block), block)
+            dst[f, r, :] = src[f, r, :].astype(bf16)
+            return 0
+
+        lax.fori_loop(0, src.shape[1] // block, body, 0)
+
+    def convert_up(l):
+        for f in order:
+            up_copy(l, f).wait()
+            convert(st_up, wu, f, min(64, dl))
+        if l + 1 < layers:
+            for f in order:
+                up_copy(l + 1, f).start()
+
+    def convert_dn(l):
+        for f in order:
+            dn_copy(l, f).wait()
+            convert(st_dn, wd, f, min(128, fq))
+        if l + 1 < layers:
+            for f in order:
+                dn_copy(l + 1, f).start()
+
+    def rs_copy(l, f, s):
+        return pltpu.make_async_remote_copy(
+            src_ref=sendb.at[f, s], dst_ref=recvb.at[l, f, s],
+            send_sem=rs_s.at[l, f, s], recv_sem=rs_r.at[l, f, s],
+            device_id={"ra": target[f]}, device_id_type=MESH,
+        )
+
+    def ag_copy(l, f, s):
+        c = wrap(p - sign[f] * (s - 1))
+        return pltpu.make_async_remote_copy(
+            src_ref=hid.at[l, c, f], dst_ref=hid.at[l, c, f],
+            send_sem=ag_s.at[l, f, s - 1], recv_sem=ag_r.at[l, f, s - 1],
+            device_id={"ra": target[f]}, device_id_type=MESH,
+        )
+
+    def ag_arrival(l, f, s):
+        c = wrap(p - sign[f] * s)
+        return pltpu.make_async_remote_copy(
+            src_ref=hid.at[l, c, f], dst_ref=hid.at[l, c, f],
+            send_sem=ag_s.at[l, f, s - 1], recv_sem=ag_r.at[l, f, s - 1],
+            device_id={"ra": target[f]}, device_id_type=MESH,
+        )
+
+    def cb_copy(l, k, c, who):
+        return pltpu.make_async_remote_copy(
+            src_ref=cbb.at[l, who, c], dst_ref=cbb.at[l, who, c],
+            send_sem=cb_s.at[l, k - 1, c], recv_sem=cb_r.at[l, k - 1, c],
+            device_id={"cb": lax.rem(cb + k, m)}, device_id_type=MESH,
+        )
+
+    def ss_copy(l, k, who):
+        return pltpu.make_async_remote_copy(
+            src_ref=ssall.at[l, who], dst_ref=ssall.at[l, who],
+            send_sem=ss_s.at[l, k - 1], recv_sem=ss_r.at[l, k - 1],
+            device_id={"ra": lax.rem(ra + k, n)}, device_id_type=MESH,
+        )
+
+    def dot(a, b):
+        return jnp.dot(a, b, preferred_element_type=f32)
+
+    for f in order:
+        up_copy(0, f).start()
+    for f in order:
+        dn_copy(0, f).start()
+
+    barrier = pltpu.get_barrier_semaphore()
+    for k in range(1, n):
+        pl.semaphore_signal(
+            barrier, inc=1, device_id={"ra": lax.rem(ra + k, n)}, device_id_type=MESH
+        )
+    for k in range(1, m):
+        pl.semaphore_signal(
+            barrier, inc=1, device_id={"cb": lax.rem(cb + k, m)}, device_id_type=MESH
+        )
+
+    def scale_in(c, _):
+        xs[c] = (tok[c].astype(f32) * pg[0:1, :]).astype(bf16)
+        return 0
+
+    lax.fori_loop(0, n, scale_in, 0)
+    pl.semaphore_wait(barrier, n + m - 2)
+
+    for l in range(layers):
+        if l == 0:
+            for f in order:
+                up_copy(l, f).wait()
+                convert(st_up, wu, f, min(64, dl))
+                sendb[f, 0] = dot(xs[wrap(p - sign[f])], wu[f]).astype(bf16)
+                rs_copy(l, f, 0).start()
+            for f in order:
+                if layers > 1:
+                    up_copy(l + 1, f).start()
+        else:
+            for f in order:
+                sendb[f, 0] = dot(xs[wrap(p - sign[f])], wu[f]).astype(bf16)
+                rs_copy(l, f, 0).start()
+        convert_dn(l)
+
+        def rs_step(s, _):
+            for f in order:
+                own[f] = dot(xs[wrap(p - sign[f] * (2 + s))], wu[f])
+            for f in order:
+                rs_copy(l, f, s).wait_recv()
+                sendb[f, s + 1] = (recvb[l, f, s].astype(f32) + own[f]).astype(bf16)
+                rs_copy(l, f, s + 1).start()
+            return 0
+
+        lax.fori_loop(0, n - 2, rs_step, 0)
+        for f in order:
+            own[f] = dot(xs[p], wu[f])
+        for f in order:
+            rs_copy(l, f, n - 2).wait_recv()
+            v = recvb[l, f, n - 2].astype(f32) + own[f]
+            v = jnp.maximum(v * us[l : l + 1, f * fq : (f + 1) * fq], 0.0)
+            hid[l, p, f] = (v * v).astype(bf16)
+            ag_copy(l, f, 1).start()
+
+        def finish(c):
+            cbb[l, cb, c] = accd[c].astype(bf16)
+            for k in range(1, m):
+                cb_copy(l, k, c, cb).start()
+
+        def zero(c, _):
+            accd[c] = jnp.zeros_like(accd[c])
+            return 0
+
+        lax.fori_loop(0, n, zero, 0)
+        a = dot(hid[l, p, 0], wd[0])
+        for f in range(1, FLOWS):
+            a = a + dot(hid[l, p, f], wd[f])
+        accd[p] = a
+        finish(p)
+        if l + 1 < layers:
+            for f in order:
+                up_copy(l + 1, f).wait()
+                convert(st_up, wu, f, min(64, dl))
+            if l + 2 < layers:
+                for f in order:
+                    up_copy(l + 2, f).start()
+
+        def ag_step(s, _):
+            for f in order:
+                ag_arrival(l, f, s).wait_recv()
+
+                @pl.when(s < n - 1)
+                def _():
+                    ag_copy(l, f, s + 1).start()
+
+            cr, cl = wrap(p - s), wrap(p + s)
+            h = FLOWS // 2
+            accd[cr] += sum(dot(hid[l, cr, f], wd[f]) for f in range(h))
+            accd[cl] += sum(dot(hid[l, cl, f], wd[f]) for f in range(h, FLOWS))
+
+            @pl.when(s >= n // 2)
+            def _():
+                finish(cr)
+
+            @pl.when(s > n // 2)
+            def _():
+                finish(cl)
+
+            return 0
+
+        lax.fori_loop(1, n, ag_step, 0)
+
+        def gather_in(c):
+            for k in range(1, m):
+                cb_copy(l, k, c, lax.rem(cb + m - k, m)).wait_recv()
+            b = cbb[l, 0, c].astype(f32)
+            for k in range(1, m):
+                b = b + cbb[l, k, c].astype(f32)
+            b = b * ds[l : l + 1, :]
+            bbuf[c] = b
+            b = b * b
+            t = b[:, :LANES]
+            for j in range(1, dl // LANES):
+                t = t + b[:, j * LANES : (j + 1) * LANES]
+            ssq[c] = t
+
+        def gather_pair(s, _):
+            gather_in(wrap(p - s))
+            gather_in(wrap(p + s))
+            return 0
+
+        gather_in(p)
+        gather_in(wrap(p + n // 2))
+        lax.fori_loop(n // 2 + 1, n, gather_pair, 0)
+
+        t = jnp.transpose(ssq[...].reshape(tokens, LANES))
+        t = jnp.sum(t, axis=0, keepdims=True)
+        ssall[l, ra] = jnp.broadcast_to(t, (8, tokens))
+        for k in range(1, n):
+            ss_copy(l, k, ra).start()
+        for k in range(1, n):
+            ss_copy(l, k, lax.rem(ra + n - k, n)).wait_recv()
+        t = ssall[l, 0]
+        for k in range(1, n):
+            t = t + ssall[l, k]
+        t = lax.rsqrt(t / (dl * n) + norm_eps)
+        t = jnp.broadcast_to(t[0:1, :], (LANES, tokens))
+        ssq[...] = jnp.transpose(t).reshape(n, rows, LANES)
+
+        before = tok if l == 0 else out
+
+        def renew(c, _):
+            inv = ssq[c]
+            for j in range(dl // LANES):
+                col = slice(j * LANES, (j + 1) * LANES)
+                branch = bbuf[c, :, col] * inv * qg[l : l + 1, col]
+                new = (residual_keep * before[c, :, col].astype(f32) + branch).astype(bf16)
+                out[c, :, col] = new
+                if l + 1 < layers:
+                    xs[c, :, col] = (new.astype(f32) * pg[l + 1 : l + 2, col]).astype(bf16)
+            return 0
+
+        lax.fori_loop(0, n, renew, 0)
+
+        def drain(s, _):
+            for f in order:
+                rs_copy(l, f, s).wait_send()
+                ag_copy(l, f, s + 1).wait_send()
+            return 0
+
+        lax.fori_loop(0, n - 1, drain, 0)
+
+        def drain_cb(c, _):
+            for k in range(1, m):
+                cb_copy(l, k, c, cb).wait_send()
+            return 0
+
+        lax.fori_loop(0, n, drain_cb, 0)
+        for k in range(1, n):
+            ss_copy(l, k, ra).wait_send()
+
+
+def local(n, m, tokens, up_weight, up_scale, down_weight, down_scale, pre_gain, post_gain):
+    t, dl = tokens.shape
+    layers, _, fl = up_weight.shape
+    fits = (
+        n % 2 == 0 and n >= 4 and m >= 2 and t % (n * BF16_ROWS) == 0 and t % LANES == 0
+        and fl % (FLOWS * LANES) == 0 and dl % LANES == 0
+    )
+    if not fits:
+        return plain(
+            tokens, up_weight, up_scale, down_weight, down_scale, pre_gain, post_gain
+        )
+    rows, fq = t // n, fl // FLOWS
+    f32, bf16 = jnp.float32, jnp.bfloat16
+    vmem = pl.BlockSpec(memory_space=pltpu.VMEM)
+    hbm = pl.BlockSpec(memory_space=pl.ANY)
+    dma = pltpu.SemaphoreType.DMA
+    out = pl.pallas_call(
+        functools.partial(kernel, n, m, layers),
+        out_shape=jax.ShapeDtypeStruct((n, rows, dl), bf16),
+        in_specs=[vmem, hbm, vmem, hbm, vmem, vmem, vmem],
+        out_specs=vmem,
+        scratch_shapes=[
+            pltpu.VMEM((FLOWS, dl, fq), f32),
+            pltpu.VMEM((FLOWS, fq, dl), f32),
+            pltpu.VMEM((FLOWS, dl, fq), bf16),
+            pltpu.VMEM((FLOWS, fq, dl), bf16),
+            pltpu.VMEM((n, rows, dl), bf16),
+            pltpu.VMEM((FLOWS, rows, fq), f32),
+            pltpu.VMEM((FLOWS, n - 1, rows, fq), bf16),
+            pltpu.VMEM((layers, FLOWS, n - 1, rows, fq), bf16),
+            pltpu.VMEM((layers, n, FLOWS, rows, fq), bf16),
+            pltpu.VMEM((n, rows, dl), f32),
+            pltpu.VMEM((layers, m, n, rows, dl), bf16),
+            pltpu.VMEM((n, rows, dl), f32),
+            pltpu.VMEM((n, rows, LANES), f32),
+            pltpu.VMEM((layers, n, 8, t), f32),
+            dma((2, FLOWS)),
+            dma((layers, FLOWS, n - 1)),
+            dma((layers, FLOWS, n - 1)),
+            dma((layers, FLOWS, n - 1)),
+            dma((layers, FLOWS, n - 1)),
+            dma((layers, m - 1, n)),
+            dma((layers, m - 1, n)),
+            dma((layers, n - 1)),
+            dma((layers, n - 1)),
+        ],
+        compiler_params=pltpu.CompilerParams(
+            collective_id=0, has_side_effects=True, vmem_limit_bytes=60 * 1024 * 1024
+        ),
+    )(
+        tokens.reshape(n, rows, dl), up_weight, up_scale, down_weight, down_scale,
+        pre_gain, post_gain,
+    )
+    return out.reshape(t, dl)
+
+
 def solution(mesh):
     return jax.shard_map(
-        local,
+        functools.partial(local, mesh.shape["ra"], mesh.shape["cb"]),
         mesh=mesh,
         in_specs=(
             P(None, "ra"),

time: 412 us -> 161 us (0.39)
  waiting for transfers between devices: 312 us -> 0 us
  Pallas kernels: 0 us -> 159 us
  blocking collectives: 42.7 us -> 0 us
  matrix products: 20.8 us -> 0 us
  other arithmetic: 20 us -> 0 us
  between operations: 13.2 us -> 0.01 us
    psum x4 -> x0, waiting for transfers between devices: 312 us -> none  [the longest x2 248 us: local(): lax.psum(partial_up.astype(jnp.bfloat16), 'ra').astype(jnp.float32)]
    pallas_call x0 -> x1, Pallas kernels: none -> 159 us  [local(): pl.pallas_call(functools.partial(kernel, n, m, layers), out_shape=jax.Sha...]
    psum x2 -> x0, blocking collectives: 42.7 us -> none  [local(): post_squares = lax.psum(jnp.sum(branch_in * branch_in, axis=1), 'ra')]
    dot_general x4 -> x0, matrix products: 20.8 us -> none  [the longest x2 11.4 us: local(): jnp.dot(hidden, down_matrix, preferred_element_type=jnp.float32)]
    another operation x2 -> x0, other arithmetic: 15.5 us -> none
  transfers between devices with their start and end apart: 4 -> 0, of which waited for: 4 -> 0; matrix products, arithmetic and copies ran while one was open for 2% -> 0% of each run, Pallas kernels for 0% -> 0%
where the time goes in v1:
time: 161 us
  Pallas kernels  159 us (99%)
  local copies, waits for them, and re-layouts  1.77 us (1%)
    pallas_call x1, Pallas kernels, local(): pl.pallas_call(functools.partial(kernel, n, m, layers), out_shape=jax.Sha...  159 us

profile of v1, /device:TPU:0, one launch (start us, length us, event | category | flops | bytes accessed | tf_op | source)
XLA Modules:
  0.0 161.3 jit_solution(2048045050633433333)
XLA Ops:
  0.0 159.5 %shard_map.73 = bf16[8,48,512]{2,1,0:T(8,128)(2,1)} custom-call(bf16[8,48,512]{2,1,0:T(8,128)(2,1)} %bitcast.3, f32[2,512,4096]{2,1,0:T(8,128)} %up.1, f32[2,4096]{1,0:T(2,128)} %us.1, f32[2,4096,512]{2,1,0:T(8,128)} %dn.1, f32[2,512]{1,0:T(2,128)} %ds.1, f32[2,512]{1,0:T(2,128)} %pg.1, f32[2,512]{1,0:T(2,128)} %qg.1), custom_call_target="tpu_custom_call" | custom-call | tf_op jit(solution)/shard_map/pallas_call | solution.py:335
  159.5 1.8 %copy.9 = bf16[384,512]{1,0:T(8,128)(2,1)} copy(bf16[384,512]{1,0:T(8,128)(2,1)} %bitcast.2) | data formatting | bytes 786432

commit v2 on v1

--- a/solution.py
+++ b/solution.py
@@ -10,7 +10,7 @@
 norm_eps = 1e-06
 residual_keep = 0.5
 MESH = pl.DeviceIdType.MESH
-FLOWS = 4
+FLOWS = 8
 LANES = 128
 BF16_ROWS = 16
 
@@ -63,7 +63,7 @@
         return 2 * q * (1 - hi) + hi * (2 * (n - 1 - q) + 1)
 
     right, left = ra_of(wrap(p + 1)), ra_of(wrap(p - 1))
-    order = [0, FLOWS // 2] + [1, FLOWS // 2 + 1]
+    order = [i + j for i in range(FLOWS // 2) for j in (0, FLOWS // 2)]
     sign = [1 if f < FLOWS // 2 else -1 for f in range(FLOWS)]
     target = [right if f < FLOWS // 2 else left for f in range(FLOWS)]
 

time: 161 us -> 160 us (level)
  no operation moved by 1% of the time
where the time goes in v2:
time: 160 us
  Pallas kernels  158 us (99%)
  local copies, waits for them, and re-layouts  1.77 us (1%)
    pallas_call x1, Pallas kernels, local(): pl.pallas_call(functools.partial(kernel, n, m, layers), out_shape=jax.Sha...  158 us

profile of v2, /device:TPU:0, one launch (start us, length us, event | category | flops | bytes accessed | tf_op | source)
XLA Modules:
  0.0 159.9 jit_solution(3243852443296518731)
XLA Ops:
  0.0 158.1 %shard_map.73 = bf16[8,48,512]{2,1,0:T(8,128)(2,1)} custom-call(bf16[8,48,512]{2,1,0:T(8,128)(2,1)} %bitcast.3, f32[2,512,4096]{2,1,0:T(8,128)} %up.1, f32[2,4096]{1,0:T(2,128)} %us.1, f32[2,4096,512]{2,1,0:T(8,128)} %dn.1, f32[2,512]{1,0:T(2,128)} %ds.1, f32[2,512]{1,0:T(2,128)} %pg.1, f32[2,512]{1,0:T(2,128)} %qg.1), custom_call_target="tpu_custom_call" | custom-call | tf_op jit(solution)/shard_map/pallas_call | solution.py:335
  158.1 1.8 %copy.9 = bf16[384,512]{1,0:T(8,128)(2,1)} copy(bf16[384,512]{1,0:T(8,128)(2,1)} %bitcast.2) | data formatting | bytes 786432
